TPU v7x, 32 devices: a whole 2x2x4 slice. The times are simulated.
32 devices in a mesh: rep: 2 (over x), fs: 4 (over z), tp: 4 (over y, core).
Axes of the slice: x: 2, y: 2, z: 4, core: 2. Of those that a mesh axis runs over, the one named last changes fastest.
Arguments:
- tokens: bfloat16 [8192, 2048], P(('rep', 'fs'), 'tp'), may hold values from -6 to 6
- mix_in_gain: bfloat16 [2048], replicated, may hold values from 0.099609375 to 1.8984375
- bgate_weight: bfloat16 [2048, 2048], P('fs', 'tp'), may hold values from -0.125 to 0.125
- cgate_weight: bfloat16 [2048, 2048], P('fs', 'tp'), may hold values from -0.125 to 0.125
- value_weight: bfloat16 [2048, 2048], P('fs', 'tp'), may hold values from -0.125 to 0.125
- conv_taps: bfloat16 [3, 2048], replicated, may hold values from -3 to 3
- out_weight: bfloat16 [2048, 2048], P('tp', 'fs'), may hold values from -0.41984465 to 0.41984465
- mix_out_gain: bfloat16 [2048], replicated, may hold values from 0.099609375 to 1.8984375
- ffn_in_gain: bfloat16 [2048], replicated, may hold values from 0.099609375 to 1.8984375
- up_weight: bfloat16 [2048, 8192], P('fs', 'tp'), may hold values from -0.125 to 0.125
- down_weight: bfloat16 [8192, 2048], P('tp', 'fs'), may hold values from -0.20992233 to 0.20992233
- ffn_out_gain: bfloat16 [2048], replicated, may hold values from 0.099609375 to 1.8984375
Outputs:
- result: bfloat16 [8192, 2048], P(('rep', 'fs'), 'tp')
All inputs are finite; a program needn't handle non-finite values.
Results may differ from a plain program's by a relative error of at most 0.02.
Values may be sent and summed in bfloat16 or wider, within the bound.
A program may use at most 128 MiB of HBM per device.

v0:
```python
import jax
import jax.numpy as jnp
from jax import lax
from jax.sharding import PartitionSpec as P

LEN = 256
epsilon = 1e-06


def normalize(rows, gain):
    rows = rows.astype(jnp.float32)
    factor = lax.rsqrt(jnp.mean(rows * rows, axis=-1, keepdims=True) + epsilon)
    return rows * factor * gain.astype(jnp.float32)


def convolve(inner, taps):
    seqs = inner.reshape(-1, LEN, inner.shape[1])
    padded = jnp.pad(seqs, ((0, 0), (1, 1), (0, 0)))
    weights = taps.astype(jnp.float32)
    out = weights[0] * padded[:, :-2] + weights[1] * padded[:, 1:-1] + weights[2] * padded[:, 2:]
    return out.reshape(inner.shape)


def body(
    tokens,
    mix_in_gain,
    bgate_weight,
    cgate_weight,
    value_weight,
    conv_taps,
    out_weight,
    mix_out_gain,
    ffn_in_gain,
    up_weight,
    down_weight,
    ffn_out_gain,
):
    column = lax.axis_index("tp")
    own_width = tokens.shape[1]
    first = column * own_width
    full_width = mix_in_gain.shape[0]
    whole = lax.all_gather(tokens, "tp", axis=1, tiled=True)
    normed = normalize(whole, mix_in_gain).astype(jnp.bfloat16)

    def add_rows(piece):
        return jnp.dot(normed, piece, preferred_element_type=jnp.float32)

    bgate = add_rows(lax.all_gather(bgate_weight, "fs", axis=0, tiled=True))
    cgate = add_rows(lax.all_gather(cgate_weight, "fs", axis=0, tiled=True))
    value = add_rows(lax.all_gather(value_weight, "fs", axis=0, tiled=True))
    bgate = bgate.astype(jnp.bfloat16)
    cgate = cgate.astype(jnp.bfloat16)
    value = value.astype(jnp.bfloat16)
    channels = bgate.shape[1]
    own_taps = lax.dynamic_slice_in_dim(conv_taps, column * channels, channels, 1)
    inner = cgate.astype(jnp.float32) * value.astype(jnp.float32)
    gated = (bgate.astype(jnp.float32) * convolve(inner, own_taps)).astype(jnp.bfloat16)
    partial_mix = jnp.dot(
        gated,
        lax.all_gather(out_weight, "fs", axis=1, tiled=True),
        preferred_element_type=jnp.float32,
    )
    mixed = lax.psum(partial_mix.astype(jnp.bfloat16), "tp").astype(jnp.float32)
    resid = (whole.astype(jnp.float32) + normalize(mixed, mix_out_gain)).astype(jnp.bfloat16)
    resid_own = lax.dynamic_slice_in_dim(resid, first, own_width, 1)
    second = normalize(resid, ffn_in_gain).astype(jnp.bfloat16)
    lifted = jnp.dot(
        second,
        lax.all_gather(up_weight, "fs", axis=0, tiled=True),
        preferred_element_type=jnp.float32,
    )
    active = jnp.square(jnp.maximum(lifted, 0.0)).astype(jnp.bfloat16)
    partial_ffn = jnp.dot(
        active,
        lax.all_gather(down_weight, "fs", axis=1, tiled=True),
        preferred_element_type=jnp.float32,
    )
    ffn = lax.psum_scatter(
        partial_ffn.astype(jnp.bfloat16), "tp", scatter_dimension=1, tiled=True
    ).astype(jnp.float32)
    ffn_energy = lax.psum(jnp.sum(ffn * ffn, axis=1), "tp")
    out_gain = lax.dynamic_slice_in_dim(ffn_out_gain, first, own_width, 0).astype(jnp.float32)
    closing = ffn * lax.rsqrt(ffn_energy[:, None] / full_width + epsilon) * out_gain
    return (resid_own.astype(jnp.float32) + closing).astype(jnp.bfloat16)


def solution(mesh):
    placed = (
        P(("rep", "fs"), "tp"),
        P(),
        P("fs", "tp"),
        P("fs", "tp"),
        P("fs", "tp"),
        P(),
        P("tp", "fs"),
        P(),
        P(),
        P("fs", "tp"),
        P("tp", "fs"),
        P(),
    )
    return jax.shard_map(
        body, mesh=mesh, in_specs=placed, out_specs=P(("rep", "fs"), "tp"), check_vma=False
    )
```

profile of v0, /device:TPU:0, one launch (start us, length us, event | category | flops | bytes accessed | tf_op | source)
XLA Modules:
  0.0 707.6 jit_solution(8818610116150277627)
XLA Ops:
  6.5 0.7 all-gather.8.cloned.1.call-update
  7.3 0.7 all-gather.12.cloned.1.call-update
  8.1 0.7 all-gather.14.cloned.1.call-update
  8.8 0.5 all-gather.10.cloned.1.call-update
  9.4 0.5 all-gather.16.cloned.1.call-update
  10.0 0.7 dynamic-slice_convert_fusion
  10.7 0.7 convert_element_type.76
  11.4 34.8 %all-gather.8.cloned.1.call-done = bf16[1024,2048]{1,0:T(8,128)(2,1)} async-done(((bf16[1024,512]{1,0:T(8,128)(2,1)}), bf16[1024,2048]{1,0:T(8,128)(2,1)}) %all-gather.8.cloned.1.call-update) | async-done | bytes 4194320 | tf_op jit(solution)/shard_map/all_gather | solution.py:42
  46.1 3.1 fusion.5
  49.2 44.2 %all-gather.12.cloned.1.call-done = bf16[2048,512]{1,0:T(8,128)(2,1)} async-done(((bf16[512,512]{1,0:T(8,128)(2,1)}), bf16[2048,512]{1,0:T(8,128)(2,1)}) %all-gather.12.cloned.1.call-update) | async-done | bytes 2097168 | tf_op jit(solution)/shard_map/all_gather | solution.py:49
  93.4 5.2 convolution_convert_fusion.2
  98.6 40.8 %all-gather.14.cloned.1.call-done = bf16[2048,512]{1,0:T(8,128)(2,1)} async-done(((bf16[512,512]{1,0:T(8,128)(2,1)}), bf16[2048,512]{1,0:T(8,128)(2,1)}) %all-gather.14.cloned.1.call-update) | async-done | bytes 2097168 | tf_op jit(solution)/shard_map/all_gather | solution.py:50
  139.4 5.2 convert_multiply_fusion.8
  144.7 0.6 multiply_add_fusion
  145.3 40.0 %all-gather.10.cloned.1.call-done = bf16[2048,512]{1,0:T(8,128)(2,1)} async-done(((bf16[512,512]{1,0:T(8,128)(2,1)}), bf16[2048,512]{1,0:T(8,128)(2,1)}) %all-gather.10.cloned.1.call-update) | async-done | bytes 2097168 | tf_op jit(solution)/shard_map/all_gather | solution.py:48
  185.4 5.2 fusion.25
  190.6 40.7 %all-gather.16.cloned.1.call-done = bf16[512,2048]{1,0:T(8,128)(2,1)} async-done(((bf16[512,512]{1,0:T(8,128)(2,1)}), bf16[512,2048]{1,0:T(8,128)(2,1)}) %all-gather.16.cloned.1.call-update) | async-done | bytes 2097168 | tf_op jit(solution)/shard_map/all_gather | solution.py:60
  231.3 5.9 convolution_convert_fusion
  237.2 0.7 all-gather.18.cloned.1.call-update
  238.0 0.7 all-gather.20.cloned.1.call-update
  238.7 0.2 reduce-scatter.2.cloned.1.call-start
  239.0 82.7 %all-reduce.3.cloned.1.call-done = bf16[1024,2048]{1,0:T(8,128)(2,1)} async-done(((bf16[1024,2048]{1,0:T(8,128)(2,1)}), bf16[1024,2048]{1,0:T(8,128)(2,1)}) %all-reduce.3.cloned.1.call-update) | async-done | bytes 4194320 | tf_op jit(solution)/shard_map/psum | solution.py:63
  321.6 3.2 fusion
  325.1 5.3 fusion.2
  330.4 142.6 %all-gather.18.cloned.1.call-done = bf16[2048,2048]{1,0:T(8,128)(2,1)} async-done(((bf16[512,2048]{1,0:T(8,128)(2,1)}), bf16[2048,2048]{1,0:T(8,128)(2,1)}) %all-gather.18.cloned.1.call-update) | async-done | bytes 8388624 | tf_op jit(solution)/shard_map/all_gather | solution.py:69
  473.0 149.4 %all-gather.20.cloned.1.call-done = bf16[2048,2048]{1,0:T(8,128)(2,1)} async-done(((bf16[2048,512]{1,0:T(8,128)(2,1)}), bf16[2048,2048]{1,0:T(8,128)(2,1)}) %all-gather.20.cloned.1.call-update) | async-done | bytes 8388624 | tf_op jit(solution)/shard_map/all_gather | solution.py:75
  622.4 25.7 %fusion.18 = bf16[1024,2048]{1,0:T(8,128)(2,1)} fusion(bf16[2048,2048]{1,0:T(8,128)(2,1)} %all-gather.20.cloned.1.call-done, bf16[2048,2048]{1,0:T(8,128)(2,1)} %all-gather.18.cloned.1.call-done, bf16[1024,2048]{1,0:T(8,128)(2,1)} %get-tuple-element.6, f32[2048]{0:T(1024)S(1)} %convert_element_type.92, f32[1024]{0:T(1024)S(1)} %add_rsqrt_fusion.1), kind=kOutput, calls=%fused_computation.22 | convolution fusion | flops 17196646400 | bytes 25178112 | tf_op jit(solution)/shard_map/dot_general | solution.py:73
  648.1 0.8 dynamic-slice_convert_fusion.1
  648.8 41.9 %reduce-scatter.2.cloned.1.call-done = bf16[1024,512]{1,0:T(8,128)(2,1)} async-done(((bf16[1024,2048]{1,0:T(8,128)(2,1)}), bf16[1024,512]{1,0:T(8,128)(2,1)}) %reduce-scatter.2.cloned.1.call-update) | async-done | bytes 1048592 | tf_op jit(solution)/shard_map/reduce_scatter | solution.py:78
  690.8 1.5 fusion.21
  692.3 5.8 psum.15
  698.1 3.0 fusion.24
  (23 shorter events, 0.6 us)
Async XLA Ops:
  6.5 39.6 %all-gather.8.cloned.1.call-start = ((), (), s32[]{:S(2)}) async-start(), calls=%async_computation.1 | async-start | bytes 5242880 | tf_op jit(solution)/shard_map/all_gather | solution.py:42
  7.3 86.1 %all-gather.12.cloned.1.call-start = ((), (), s32[]{:S(2)}) async-start(), calls=%async_computation.3 | async-start | bytes 2621440 | tf_op jit(solution)/shard_map/all_gather | solution.py:49
  8.0 131.4 %all-gather.14.cloned.1.call-start = ((), (), s32[]{:S(2)}) async-start(), calls=%async_computation.4 | async-start | bytes 2621440 | tf_op jit(solution)/shard_map/all_gather | solution.py:50
  8.7 176.6 %all-gather.10.cloned.1.call-start = ((), (), s32[]{:S(2)}) async-start(), calls=%async_computation.2 | async-start | bytes 2621440 | tf_op jit(solution)/shard_map/all_gather | solution.py:48
  9.3 221.9 %all-gather.16.cloned.1.call-start = ((), (), s32[]{:S(2)}) async-start(), calls=%async_computation.5 | async-start | bytes 2621440 | tf_op jit(solution)/shard_map/all_gather | solution.py:60
  9.9 311.7 %all-reduce.3.cloned.1.call-start = ((), (), s32[]{:S(2)}) async-start(), calls=%async_computation.6 | async-start | bytes 8388608 | tf_op jit(solution)/shard_map/psum | solution.py:63
  237.2 1.8 copy-start.1
  237.2 1.8 copy-start.2
  237.2 235.8 %all-gather.18.cloned.1.call-start = ((), (), s32[]{:S(2)}) async-start(), calls=%async_computation.7 | async-start | bytes 10485760 | tf_op jit(solution)/shard_map/all_gather | solution.py:69
  237.9 384.4 %all-gather.20.cloned.1.call-start = ((), (), s32[]{:S(2)}) async-start(), calls=%async_computation.8 | async-start | bytes 10485760 | tf_op jit(solution)/shard_map/all_gather | solution.py:75
  238.7 452.1 %reduce-scatter.2.cloned.1.call-start = ((), (), s32[]{:S(2)}) async-start(), calls=%async_computation.9 | async-start | bytes 5242880 | tf_op jit(solution)/shard_map/reduce_scatter | solution.py:78
  321.6 3.4 copy-start
Sparse Core Ops, SparseCore 0:
  8.9 37.1 all-gather.7
  47.7 45.6 all-gather.11
  94.9 44.4 all-gather.13
  140.9 44.4 all-gather.9
  186.8 44.4 all-gather.15
  237.3 84.2 all-reduce.2
  323.2 149.7 all-gather.17
  474.6 147.7 all-gather.19
  648.2 42.5 reduce-scatter.1
where the time goes:
time: 708 us
  waiting for transfers between devices  622 us (88%)
  matrix products  47.3 us (7%)
  other arithmetic  18.9 us (3%)
  between operations  13.3 us (2%)
    all_gather x1, waiting for transfers between devices, body(): lax.all_gather(down_weight, 'fs', axis=1, tiled=True)  149 us
    all_gather x1, waiting for transfers between devices, body(): lax.all_gather(up_weight, 'fs', axis=0, tiled=True)  143 us
    psum x1, waiting for transfers between devices, body(): mixed = lax.psum(partial_mix.astype(jnp.bfloat16), 'tp').astype(jnp.float32)  82.7 us
    all_gather x1, waiting for transfers between devices, body(): cgate = add_rows(lax.all_gather(cgate_weight, 'fs', axis=0, tiled=True))  44.2 us
    reduce_scatter x1, waiting for transfers between devices, body(): lax.psum_scatter(partial_ffn.astype(jnp.bfloat16), 'tp', scatter_dimensio...  41.9 us
    all_gather x1, waiting for transfers between devices, body(): value = add_rows(lax.all_gather(value_weight, 'fs', axis=0, tiled=True))  40.8 us
    all_gather x1, waiting for transfers between devices, body(): lax.all_gather(out_weight, 'fs', axis=1, tiled=True)  40.7 us
    all_gather x1, waiting for transfers between devices, body(): bgate = add_rows(lax.all_gather(bgate_weight, 'fs', axis=0, tiled=True))  40 us
  transfers between devices with their start and end apart: 9, of which 9 were waited for; matrix products, arithmetic and copies ran while one was open for 4% of the time, Pallas kernels for 0%

commit v1 on v0

--- a/solution.py
+++ b/solution.py
@@ -60,7 +60,9 @@
         lax.all_gather(out_weight, "fs", axis=1, tiled=True),
         preferred_element_type=jnp.float32,
     )
-    mixed = lax.psum(partial_mix.astype(jnp.bfloat16), "tp").astype(jnp.float32)
+    mixed = jnp.sum(lax.all_gather(partial_mix.astype(jnp.bfloat16), "tp"), axis=0).astype(
+        jnp.float32
+    )
     resid = (whole.astype(jnp.float32) + normalize(mixed, mix_out_gain)).astype(jnp.bfloat16)
     resid_own = lax.dynamic_slice_in_dim(resid, first, own_width, 1)
     second = normalize(resid, ffn_in_gain).astype(jnp.bfloat16)

time: 708 us -> 728 us (1.028)
  other arithmetic: 18.9 us -> 31.7 us
    all_gather x0 -> x1, waiting for transfers between devices: none -> 103 us  [body(): lax.all_gather(partial_mix.astype(jnp.bfloat16), 'tp')]
    psum x1 -> x0, waiting for transfers between devices: 82.7 us -> none  [body(): mixed = lax.psum(partial_mix.astype(jnp.bfloat16), 'tp').astype(jnp.float32)]
    all_gather x1, waiting for transfers between devices: 143 us -> 129 us  [body(): lax.all_gather(up_weight, 'fs', axis=0, tiled=True)]
    reduce_sum x0 -> x1, other arithmetic: none -> 12.3 us  [body(): jnp.sum(lax.all_gather(partial_mix.astype(jnp.bfloat16), 'tp'), axis=0)]
  transfers between devices with their start and end apart: 9 -> 9, of which waited for: 9 -> 9; matrix products, arithmetic and copies ran while one was open for 4% -> 6% of each run, Pallas kernels for 0% -> 0%
where the time goes in v1:
time: 728 us
  waiting for transfers between devices  629 us (86%)
  matrix products  47.3 us (6%)
  other arithmetic  31.7 us (4%)
  between operations  13.3 us (2%)
    all_gather x1, waiting for transfers between devices, body(): lax.all_gather(down_weight, 'fs', axis=1, tiled=True)  149 us
    all_gather x1, waiting for transfers between devices, body(): lax.all_gather(up_weight, 'fs', axis=0, tiled=True)  129 us
    all_gather x1, waiting for transfers between devices, body(): lax.all_gather(partial_mix.astype(jnp.bfloat16), 'tp')  103 us
    all_gather x1, waiting for transfers between devices, body(): cgate = add_rows(lax.all_gather(cgate_weight, 'fs', axis=0, tiled=True))  44.2 us
    reduce_scatter x1, waiting for transfers between devices, body(): lax.psum_scatter(partial_ffn.astype(jnp.bfloat16), 'tp', scatter_dimensio...  42 us
    all_gather x1, waiting for transfers between devices, body(): value = add_rows(lax.all_gather(value_weight, 'fs', axis=0, tiled=True))  40.8 us
    all_gather x1, waiting for transfers between devices, body(): lax.all_gather(out_weight, 'fs', axis=1, tiled=True)  40.7 us
    all_gather x1, waiting for transfers between devices, body(): bgate = add_rows(lax.all_gather(bgate_weight, 'fs', axis=0, tiled=True))  40 us
  transfers between devices with their start and end apart: 9, of which 9 were waited for; matrix products, arithmetic and copies ran while one was open for 6% of the time, Pallas kernels for 0%

profile of v1, /device:TPU:0, one launch (start us, length us, event | category | flops | bytes accessed | tf_op | source)
XLA Modules:
  0.0 727.9 jit_solution(17972093765376538032)
XLA Ops:
  6.5 0.7 all-gather.10.cloned.1.call-update
  7.3 0.7 all-gather.14.cloned.1.call-update
  8.1 0.7 all-gather.16.cloned.1.call-update
  8.8 0.5 all-gather.12.cloned.1.call-update
  9.4 0.5 all-gather.18.cloned.1.call-update
  10.0 0.7 dynamic-slice_convert_fusion
  10.7 0.7 convert_element_type.78
  11.4 34.8 %all-gather.10.cloned.1.call-done = bf16[1024,2048]{1,0:T(8,128)(2,1)} async-done(((bf16[1024,512]{1,0:T(8,128)(2,1)}), bf16[1024,2048]{1,0:T(8,128)(2,1)}) %all-gather.10.cloned.1.call-update) | async-done | bytes 4194320 | tf_op jit(solution)/shard_map/all_gather | solution.py:42
  46.1 3.1 fusion.5
  49.2 44.2 %all-gather.14.cloned.1.call-done = bf16[2048,512]{1,0:T(8,128)(2,1)} async-done(((bf16[512,512]{1,0:T(8,128)(2,1)}), bf16[2048,512]{1,0:T(8,128)(2,1)}) %all-gather.14.cloned.1.call-update) | async-done | bytes 2097168 | tf_op jit(solution)/shard_map/all_gather | solution.py:49
  93.4 5.2 convolution_convert_fusion.2
  98.6 40.8 %all-gather.16.cloned.1.call-done = bf16[2048,512]{1,0:T(8,128)(2,1)} async-done(((bf16[512,512]{1,0:T(8,128)(2,1)}), bf16[2048,512]{1,0:T(8,128)(2,1)}) %all-gather.16.cloned.1.call-update) | async-done | bytes 2097168 | tf_op jit(solution)/shard_map/all_gather | solution.py:50
  139.4 5.2 convert_multiply_fusion.8
  144.7 0.6 multiply_add_fusion
  145.3 40.0 %all-gather.12.cloned.1.call-done = bf16[2048,512]{1,0:T(8,128)(2,1)} async-done(((bf16[512,512]{1,0:T(8,128)(2,1)}), bf16[2048,512]{1,0:T(8,128)(2,1)}) %all-gather.12.cloned.1.call-update) | async-done | bytes 2097168 | tf_op jit(solution)/shard_map/all_gather | solution.py:48
  185.4 5.2 fusion.25
  190.6 40.7 %all-gather.18.cloned.1.call-done = bf16[512,2048]{1,0:T(8,128)(2,1)} async-done(((bf16[512,512]{1,0:T(8,128)(2,1)}), bf16[512,2048]{1,0:T(8,128)(2,1)}) %all-gather.18.cloned.1.call-update) | async-done | bytes 2097168 | tf_op jit(solution)/shard_map/all_gather | solution.py:60
  231.3 5.9 convolution_convert_fusion
  237.2 0.7 all-gather.20.cloned.1.call-update
  238.0 0.7 all-gather.22.cloned.1.call-update
  239.0 103.1 %all-gather.24.cloned.1.call-done = bf16[4096,2048]{1,0:T(8,128)(2,1)} async-done(((bf16[1024,2048]{1,0:T(8,128)(2,1)}), bf16[4096,2048]{1,0:T(8,128)(2,1)}) %all-gather.24.cloned.1.call-update) | async-done | bytes 16777232 | tf_op jit(solution)/shard_map/all_gather | solution.py:63
  342.0 12.3 %reduce_sum.49 = bf16[1024,2048]{1,0:T(8,128)(2,1)} reduce(bf16[4,1024,2048]{2,1,0:T(8,128)(2,1)} %bitcast.16, bf16[]{:T(256)} %constant.23.clone.1), dimensions={0}, to_apply=%region_1.2 | reduce | flops 6291456 | bytes 20971522 | tf_op jit(solution)/shard_map/reduce_sum | solution.py:63
  354.3 3.6 fusion
  358.4 5.4 fusion.2
  363.8 129.4 %all-gather.20.cloned.1.call-done = bf16[2048,2048]{1,0:T(8,128)(2,1)} async-done(((bf16[512,2048]{1,0:T(8,128)(2,1)}), bf16[2048,2048]{1,0:T(8,128)(2,1)}) %all-gather.20.cloned.1.call-update) | async-done | bytes 8388624 | tf_op jit(solution)/shard_map/all_gather | solution.py:71
  493.3 149.4 %all-gather.22.cloned.1.call-done = bf16[2048,2048]{1,0:T(8,128)(2,1)} async-done(((bf16[2048,512]{1,0:T(8,128)(2,1)}), bf16[2048,2048]{1,0:T(8,128)(2,1)}) %all-gather.22.cloned.1.call-update) | async-done | bytes 8388624 | tf_op jit(solution)/shard_map/all_gather | solution.py:77
  642.7 25.7 %fusion.18 = bf16[1024,2048]{1,0:T(8,128)(2,1)} fusion(bf16[2048,2048]{1,0:T(8,128)(2,1)} %all-gather.22.cloned.1.call-done, bf16[2048,2048]{1,0:T(8,128)(2,1)} %all-gather.20.cloned.1.call-done, bf16[1024,2048]{1,0:T(8,128)(2,1)} %get-tuple-element.6, f32[2048]{0:T(1024)S(1)} %convert_element_type.94, f32[1024]{0:T(1024)S(1)} %add_rsqrt_fusion.1), kind=kOutput, calls=%fused_computation.22 | convolution fusion | flops 17196646400 | bytes 25178112 | tf_op jit(solution)/shard_map/dot_general | solution.py:75
  668.3 0.8 dynamic-slice_convert_fusion.1
  669.1 42.0 %reduce-scatter.2.cloned.1.call-done = bf16[1024,512]{1,0:T(8,128)(2,1)} async-done(((bf16[1024,2048]{1,0:T(8,128)(2,1)}), bf16[1024,512]{1,0:T(8,128)(2,1)}) %reduce-scatter.2.cloned.1.call-update) | async-done | bytes 1048592 | tf_op jit(solution)/shard_map/reduce_scatter | solution.py:80
  711.1 1.5 fusion.21
  712.6 5.8 psum.7
  718.4 3.0 fusion.24
  (24 shorter events, 1.0 us)
Async XLA Ops:
  6.5 39.6 %all-gather.10.cloned.1.call-start = ((), (), s32[]{:S(2)}) async-start(), calls=%async_computation.1 | async-start | bytes 5242880 | tf_op jit(solution)/shard_map/all_gather | solution.py:42
  7.3 86.1 %all-gather.14.cloned.1.call-start = ((), (), s32[]{:S(2)}) async-start(), calls=%async_computation.3 | async-start | bytes 2621440 | tf_op jit(solution)/shard_map/all_gather | solution.py:49
  8.0 131.4 %all-gather.16.cloned.1.call-start = ((), (), s32[]{:S(2)}) async-start(), calls=%async_computation.4 | async-start | bytes 2621440 | tf_op jit(solution)/shard_map/all_gather | solution.py:50
  8.7 176.6 %all-gather.12.cloned.1.call-start = ((), (), s32[]{:S(2)}) async-start(), calls=%async_computation.2 | async-start | bytes 2621440 | tf_op jit(solution)/shard_map/all_gather | solution.py:48
  9.3 221.9 %all-gather.18.cloned.1.call-start = ((), (), s32[]{:S(2)}) async-start(), calls=%async_computation.5 | async-start | bytes 2621440 | tf_op jit(solution)/shard_map/all_gather | solution.py:60
  9.9 332.1 %all-gather.24.cloned.1.call-start = ((), (), s32[]{:S(2)}) async-start(), calls=%async_computation.9 | async-start | bytes 20971520 | tf_op jit(solution)/shard_map/all_gather | solution.py:63
  237.2 1.8 copy-start.1
  237.2 1.8 copy-start.2
  237.2 256.1 %all-gather.20.cloned.1.call-start = ((), (), s32[]{:S(2)}) async-start(), calls=%async_computation.6 | async-start | bytes 10485760 | tf_op jit(solution)/shard_map/all_gather | solution.py:71
  237.9 404.7 %all-gather.22.cloned.1.call-start = ((), (), s32[]{:S(2)}) async-start(), calls=%async_computation.7 | async-start | bytes 10485760 | tf_op jit(solution)/shard_map/all_gather | solution.py:77
  238.7 472.4 %reduce-scatter.2.cloned.1.call-start = ((), (), s32[]{:S(2)}) async-start(), calls=%async_computation.8 | async-start | bytes 5242880 | tf_op jit(solution)/shard_map/reduce_scatter | solution.py:80
  354.3 4.1 copy-start
Sparse Core Ops, SparseCore 0:
  8.9 37.1 all-gather.9
  47.7 45.6 all-gather.13
  94.9 44.4 all-gather.15
  140.9 44.4 all-gather.11
  186.8 44.4 all-gather.17
  237.3 104.6 all-gather.23
  343.6 149.5 all-gather.19
  494.8 147.7 all-gather.21
  668.5 42.5 reduce-scatter.1
